TPU v7x, 32 devices: a whole 2x2x4 slice. The times are simulated.
32 devices in a mesh: rep: 1, fs: 8 (over z, y), tp: 4 (over x, core).
Axes of the slice: x: 2, y: 2, z: 4, core: 2. Of those that a mesh axis runs over, the one named last changes fastest.
Arguments:
- tokens: bfloat16 [4096, 2048], P(('rep', 'fs')), may hold values from -6 to 6
- gate_outer: bfloat16 [2048, 1024], P('fs', 'tp'), may hold values from -0.125 to 0.125
- gate_inner: bfloat16 [2048, 1024], P('fs', 'tp'), may hold values from -0.125 to 0.125
- conv_input: bfloat16 [2048, 1024], P('fs', 'tp'), may hold values from -0.125 to 0.125
- mixer_output: bfloat16 [2048, 1024], P('fs', 'tp'), may hold values from -0.1875 to 0.1875
- conv_taps: float32 [3, 1024], P(None, 'tp'), may hold values from -3 to 3
- mixer_gain: float32 [2048], replicated, may hold values from 0.1 to 1.9
- mixer_shift: float32 [2048], replicated, may hold values from -3 to 3
- up_weight: bfloat16 [2048, 8192], P('fs', 'tp'), may hold values from -0.125 to 0.125
- down_weight: bfloat16 [2048, 8192], P('fs', 'tp'), may hold values from -0.0625 to 0.0625
- channel_gain: float32 [2048], replicated, may hold values from 0.1 to 1.9
- channel_shift: float32 [2048], replicated, may hold values from -3 to 3
Outputs:
- mixed: bfloat16 [4096, 2048], P(('rep', 'fs'))
All inputs are finite; a program needn't handle non-finite values.
Results may differ from a plain program's by a relative error of at most 0.014.
Values may be sent and summed in bfloat16 or wider, within the bound.
A program may use at most 64 MiB of HBM per device.

v0:
```python
import jax
import jax.numpy as jnp
from jax import lax
from jax.sharding import PartitionSpec as P

residual_scale = 8.0**0.25
norm_epsilon = 1e-05


def layer_norm(values, gain, shift):
    row_mean = jnp.mean(values, -1, keepdims=True)
    centered = values - row_mean
    variance = jnp.mean(centered * centered, -1, keepdims=True)
    return centered * lax.rsqrt(variance + norm_epsilon) * gain + shift


def rounded_partial(left, right_t):
    product = lax.dot_general(
        left, right_t, (((1,), (1,)), ((), ())), preferred_element_type=jnp.float32
    )
    return lax.optimization_barrier(product.astype(jnp.bfloat16)).astype(jnp.float32)


def gated_conv(outer_gate, inner_gate, conv_values, conv_taps):
    seq_len = conv_values.shape[0]
    tap_count = conv_taps.shape[0]
    product = inner_gate * conv_values
    padded = jnp.pad(product, ((tap_count - 1, 0), (0, 0)))
    result = jnp.zeros_like(product)
    for tap_index in range(tap_count):
        result = result + conv_taps[tap_index] * padded[tap_index : tap_index + seq_len]
    return (outer_gate * result).astype(jnp.bfloat16)


def local(
    tokens,
    gate_outer,
    gate_inner,
    conv_input,
    mixer_output,
    conv_taps,
    mixer_gain,
    mixer_shift,
    up_weight,
    down_weight,
    channel_gain,
    channel_shift,
):
    seq_len = tokens.shape[0]
    own_rows = seq_len // lax.axis_size("tp")
    own_start = lax.axis_index("tp") * own_rows
    columns = tokens
    outer_gate = jnp.dot(
        columns,
        lax.all_gather(gate_outer, "fs", axis=0, tiled=True),
        preferred_element_type=jnp.float32,
    )
    inner_gate = jnp.dot(
        columns,
        lax.all_gather(gate_inner, "fs", axis=0, tiled=True),
        preferred_element_type=jnp.float32,
    )
    conv_values = jnp.dot(
        columns,
        lax.all_gather(conv_input, "fs", axis=0, tiled=True),
        preferred_element_type=jnp.float32,
    )
    output_weight = lax.all_gather(mixer_output, "fs", axis=0, tiled=True)
    conv_out = gated_conv(outer_gate, inner_gate, conv_values, conv_taps)
    mixer_sum = lax.psum(
        rounded_partial(conv_out, output_weight).astype(jnp.bfloat16), "tp"
    ).astype(jnp.float32)
    first_rows = layer_norm(
        residual_scale * tokens.astype(jnp.float32) + mixer_sum, mixer_gain, mixer_shift
    ).astype(jnp.bfloat16)
    first_own = lax.dynamic_slice_in_dim(first_rows, own_start, own_rows, 0)
    columns = first_rows
    up_product = jnp.dot(
        columns,
        lax.all_gather(up_weight, "fs", axis=0, tiled=True),
        preferred_element_type=jnp.float32,
    )
    down_full = lax.all_gather(down_weight, "fs", axis=0, tiled=True)
    hidden = jnp.square(jax.nn.relu(up_product)).astype(jnp.bfloat16)
    channel_sum = lax.psum_scatter(
        rounded_partial(hidden, down_full).astype(jnp.bfloat16),
        "tp",
        scatter_dimension=0,
        tiled=True,
    ).astype(jnp.float32)
    output_own = layer_norm(
        residual_scale * first_own.astype(jnp.float32) + channel_sum, channel_gain, channel_shift
    ).astype(jnp.bfloat16)
    return lax.all_gather(output_own, "tp", axis=0, tiled=True)


def solution(mesh):
    in_specs = (
        P(("rep", "fs"), None),
        P("fs", "tp"),
        P("fs", "tp"),
        P("fs", "tp"),
        P("fs", "tp"),
        P(None, "tp"),
        P(),
        P(),
        P("fs", "tp"),
        P("fs", "tp"),
        P(),
        P(),
    )
    out_specs = P(("rep", "fs"), None)
    return jax.shard_map(local, mesh=mesh, in_specs=in_specs, out_specs=out_specs, check_vma=False)
```

profile of v0, /device:TPU:0, one launch (start us, length us, event | category | flops | bytes accessed | tf_op | source)
XLA Modules:
  0.0 565.9 jit_solution(9245024707025191946)
XLA Ops:
  6.5 0.7 all-gather.10.cloned.1.call-update
  7.3 0.0 all-gather.12.cloned.1.call-start
  7.3 0.7 all-gather.12.cloned.1.call-update
  8.1 0.7 all-gather.14.cloned.1.call-update
  8.8 0.5 all-gather.8.cloned.1.call-update
  9.3 0.0 all-reduce.3.cloned.1.call-start
  9.4 0.8 fusion.16
  10.2 42.3 %all-gather.10.cloned.1.call-done = bf16[2048,256]{1,0:T(8,128)(2,1)} async-done(((bf16[256,256]{1,0:T(8,128)(2,1)}), bf16[2048,256]{1,0:T(8,128)(2,1)}) %all-gather.10.cloned.1.call-update) | async-done | bytes 1048592 | tf_op jit(solution)/shard_map/all_gather | solution.py:60
  52.5 2.6 fusion.17
  55.1 38.6 %all-gather.12.cloned.1.call-done = bf16[2048,256]{1,0:T(8,128)(2,1)} async-done(((bf16[256,256]{1,0:T(8,128)(2,1)}), bf16[2048,256]{1,0:T(8,128)(2,1)}) %all-gather.12.cloned.1.call-update) | async-done | bytes 1048592 | tf_op jit(solution)/shard_map/all_gather | solution.py:65
  93.6 1.9 convolution_multiply_fusion
  95.6 39.2 %all-gather.14.cloned.1.call-done = bf16[2048,256]{1,0:T(8,128)(2,1)} async-done(((bf16[256,256]{1,0:T(8,128)(2,1)}), bf16[2048,256]{1,0:T(8,128)(2,1)}) %all-gather.14.cloned.1.call-update) | async-done | bytes 1048592 | tf_op jit(solution)/shard_map/all_gather | solution.py:68
  134.8 41.0 %all-gather.8.cloned.1.call-done = bf16[2048,256]{1,0:T(8,128)(2,1)} async-done(((bf16[256,256]{1,0:T(8,128)(2,1)}), bf16[2048,256]{1,0:T(8,128)(2,1)}) %all-gather.8.cloned.1.call-update) | async-done | bytes 1048592 | tf_op jit(solution)/shard_map/all_gather | solution.py:55
  175.8 5.2 convolution_convert_fusion
  181.0 0.0 all-gather.16.cloned.1.call-start
  181.0 0.5 all-gather.16.cloned.1.call-update
  181.6 0.7 all-gather.18.cloned.1.call-update
  182.3 0.2 reduce-scatter.2.cloned.1.call-start
  182.6 48.7 %all-reduce.3.cloned.1.call-done = bf16[512,2048]{1,0:T(8,128)(2,1)} async-done(((bf16[512,2048]{1,0:T(8,128)(2,1)}), bf16[512,2048]{1,0:T(8,128)(2,1)}) %all-reduce.3.cloned.1.call-update) | async-done | bytes 2097168 | tf_op jit(solution)/shard_map/psum | solution.py:70
  231.2 2.5 fusion
  233.7 1.0 multiply_reduce_fusion
  234.8 2.5 add_convert_fusion
  237.3 120.5 %all-gather.16.cloned.1.call-done = bf16[2048,2048]{1,0:T(8,128)(2,1)} async-done(((bf16[256,2048]{1,0:T(8,128)(2,1)}), bf16[2048,2048]{1,0:T(8,128)(2,1)}) %all-gather.16.cloned.1.call-update) | async-done | bytes 8388624 | tf_op jit(solution)/shard_map/all_gather | solution.py:80
  357.8 124.8 %all-gather.18.cloned.1.call-done = bf16[2048,2048]{1,0:T(8,128)(2,1)} async-done(((bf16[256,2048]{1,0:T(8,128)(2,1)}), bf16[2048,2048]{1,0:T(8,128)(2,1)}) %all-gather.18.cloned.1.call-update) | async-done | bytes 8388624 | tf_op jit(solution)/shard_map/all_gather | solution.py:83
  482.6 16.5 %convolution_convert_fusion.1 = bf16[512,2048]{1,0:T(8,128)(2,1)} fusion(bf16[2048,2048]{1,0:T(8,128)(2,1)} %all-gather.18.cloned.1.call-done, bf16[512,2048]{1,0:T(8,128)(2,1)} %add_convert_fusion, bf16[2048,2048]{1,0:T(8,128)(2,1)} %all-gather.16.cloned.1.call-done), kind=kOutput, calls=%fused_computation.6 | convolution fusion | flops 8594128896 | bytes 20971520 | tf_op jit(solution)/shard_map/dot_general | solution.py:18
  499.2 0.0 all-gather.20.cloned.1.call-start
  499.2 29.4 %reduce-scatter.2.cloned.1.call-done = bf16[128,2048]{1,0:T(8,128)(2,1)} async-done(((bf16[512,2048]{1,0:T(8,128)(2,1)}), bf16[128,2048]{1,0:T(8,128)(2,1)}) %reduce-scatter.2.cloned.1.call-update) | async-done | bytes 524304 | tf_op jit(solution)/shard_map/reduce_scatter | solution.py:85
  528.6 1.3 fusion.2
  529.9 1.4 multiply_reduce_fusion.1
  531.3 2.2 add_convert_fusion.1
  533.5 22.7 %all-gather.20.cloned.1.call-done = bf16[512,2048]{1,0:T(8,128)(2,1)} async-done(((bf16[128,2048]{1,0:T(8,128)(2,1)}), bf16[512,2048]{1,0:T(8,128)(2,1)}) %all-gather.20.cloned.1.call-update) | async-done | bytes 2097168 | tf_op jit(solution)/shard_map/all_gather | solution.py:94
  556.3 3.2 copy.15
  (25 shorter events, 0.2 us)
Async XLA Ops:
  6.5 87.1 %copy-start = (bf16[512,2048]{1,0:T(8,128)(2,1)S(1)}, bf16[512,2048]{1,0:T(8,128)(2,1)}, u32[]{:S(2)}) copy-start(bf16[512,2048]{1,0:T(8,128)(2,1)} %param.12) | copy-start | bytes 6291460
  6.5 46.0 %all-gather.10.cloned.1.call-start = ((), (), s32[]{:S(2)}) async-start(), calls=%async_computation.2 | async-start | bytes 1179648 | tf_op jit(solution)/shard_map/all_gather | solution.py:60
  7.3 86.4 %all-gather.12.cloned.1.call-start = ((), (), s32[]{:S(2)}) async-start(), calls=%async_computation.3 | async-start | bytes 1179648 | tf_op jit(solution)/shard_map/all_gather | solution.py:65
  8.0 126.8 %all-gather.14.cloned.1.call-start = ((), (), s32[]{:S(2)}) async-start(), calls=%async_computation.4 | async-start | bytes 1179648 | tf_op jit(solution)/shard_map/all_gather | solution.py:68
  8.7 167.1 %all-gather.8.cloned.1.call-start = ((), (), s32[]{:S(2)}) async-start(), calls=%async_computation.1 | async-start | bytes 1179648 | tf_op jit(solution)/shard_map/all_gather | solution.py:55
  9.3 221.9 %all-reduce.3.cloned.1.call-start = ((), (), s32[]{:S(2)}) async-start(), calls=%async_computation.5 | async-start | bytes 4194304 | tf_op jit(solution)/shard_map/psum | solution.py:70
  181.0 176.8 %all-gather.16.cloned.1.call-start = ((), (), s32[]{:S(2)}) async-start(), calls=%async_computation.6 | async-start | bytes 9437184 | tf_op jit(solution)/shard_map/all_gather | solution.py:80
  181.6 301.0 %all-gather.18.cloned.1.call-start = ((), (), s32[]{:S(2)}) async-start(), calls=%async_computation.7 | async-start | bytes 9437184 | tf_op jit(solution)/shard_map/all_gather | solution.py:83
  182.3 52.4 %copy-start.3 = (f32[2048]{0:T(1024)S(1)}, f32[2048]{0:T(1024)}, u32[]{:S(2)}) copy-start(f32[2048]{0:T(1024)} %param.19) | copy-start | bytes 24580
  182.3 52.4 %copy-start.4 = (f32[2048]{0:T(1024)S(1)}, f32[2048]{0:T(1024)}, u32[]{:S(2)}) copy-start(f32[2048]{0:T(1024)} %param.18) | copy-start | bytes 24580
  182.3 346.3 %reduce-scatter.2.cloned.1.call-start = ((), (), s32[]{:S(2)}) async-start(), calls=%async_computation.8 | async-start | bytes 2621440 | tf_op jit(solution)/shard_map/reduce_scatter | solution.py:85
  231.2 2.5 copy-start.1
  237.3 291.4 %copy-start.2 = (bf16[512,2048]{1,0:T(8,128)(2,1)S(1)}, bf16[512,2048]{1,0:T(8,128)(2,1)}, u32[]{:S(2)}) copy-start(bf16[512,2048]{1,0:T(8,128)(2,1)} %add_convert_fusion) | copy-start | bytes 6291460
  499.1 32.2 %copy-start.5 = (f32[2048]{0:T(1024)S(1)}, f32[2048]{0:T(1024)}, u32[]{:S(2)}) copy-start(f32[2048]{0:T(1024)} %param.23) | copy-start | bytes 24580
  499.1 32.2 %copy-start.6 = (f32[2048]{0:T(1024)S(1)}, f32[2048]{0:T(1024)}, u32[]{:S(2)}) copy-start(f32[2048]{0:T(1024)} %param.22) | copy-start | bytes 24580
  499.2 57.1 %all-gather.20.cloned.1.call-start = ((), (), s32[]{:S(2)}) async-start(), calls=%async_computation.9 | async-start | bytes 2621440 | tf_op jit(solution)/shard_map/all_gather | solution.py:94
Sparse Core Ops, SparseCore 0:
  9.5 42.9 all-gather.9
  54.6 38.9 all-gather.11
  95.8 38.9 all-gather.13
  136.8 38.9 all-gather.7
  181.1 50.0 all-reduce.2
  233.2 124.5 all-gather.15
  359.9 122.6 all-gather.17
  499.3 29.3 reduce-scatter.1
  533.6 22.5 all-gather.19
where the time goes:
time: 566 us
  waiting for transfers between devices  511 us (90%)
  matrix products  26.2 us (5%)
  between operations  13.3 us (2%)
  other arithmetic  10.9 us (2%)
    all_gather x1, waiting for transfers between devices, local(): down_full = lax.all_gather(down_weight, 'fs', axis=0, tiled=True)  125 us
    all_gather x1, waiting for transfers between devices, local(): lax.all_gather(up_weight, 'fs', axis=0, tiled=True)  121 us
    psum x1, waiting for transfers between devices, local(): lax.psum(rounded_partial(conv_out, output_weight).astype(jnp.bfloat16), '...  48.7 us
    all_gather x1, waiting for transfers between devices, local(): lax.all_gather(gate_inner, 'fs', axis=0, tiled=True)  42.3 us
    all_gather x1, waiting for transfers between devices, local(): lax.all_gather(gate_outer, 'fs', axis=0, tiled=True)  41 us
    all_gather x1, waiting for transfers between devices, local(): output_weight = lax.all_gather(mixer_output, 'fs', axis=0, tiled=True)  39.2 us
    all_gather x1, waiting for transfers between devices, local(): lax.all_gather(conv_input, 'fs', axis=0, tiled=True)  38.6 us
    reduce_scatter x1, waiting for transfers between devices, local(): lax.psum_scatter(rounded_partial(hidden, down_full).astype(jnp.bfloat16),...  29.4 us
  transfers between devices with their start and end apart: 9, of which 9 were waited for; matrix products, arithmetic and copies ran while one was open for 2% of the time, Pallas kernels for 0%

commit v1 on v0

--- a/solution.py
+++ b/solution.py
@@ -67,8 +67,8 @@
     )
     output_weight = lax.all_gather(mixer_output, "fs", axis=0, tiled=True)
     conv_out = gated_conv(outer_gate, inner_gate, conv_values, conv_taps)
-    mixer_sum = lax.psum(
-        rounded_partial(conv_out, output_weight).astype(jnp.bfloat16), "tp"
+    mixer_sum = jnp.sum(
+        lax.all_gather(rounded_partial(conv_out, output_weight).astype(jnp.bfloat16), "tp"), axis=0
     ).astype(jnp.float32)
     first_rows = layer_norm(
         residual_scale * tokens.astype(jnp.float32) + mixer_sum, mixer_gain, mixer_shift

time: 566 us -> 573 us (1.012)
  other arithmetic: 10.9 us -> 18.1 us
    all_gather x0 -> x1, waiting for transfers between devices: none -> 55.6 us  [local(): lax.all_gather(rounded_partial(conv_out, output_weight).astype(jnp.bfloat...]
    psum x1 -> x0, waiting for transfers between devices: 48.7 us -> none  [local(): lax.psum(rounded_partial(conv_out, output_weight).astype(jnp.bfloat16), '...]
    all_gather x1, waiting for transfers between devices: 121 us -> 113 us  [local(): lax.all_gather(up_weight, 'fs', axis=0, tiled=True)]
    reduce_sum x0 -> x1, other arithmetic: none -> 7.2 us  [local(): jnp.sum(lax.all_gather(rounded_partial(conv_out, output_weight).astype(jn...]
  transfers between devices with their start and end apart: 9 -> 9, of which waited for: 9 -> 9; matrix products, arithmetic and copies ran while one was open for 2% -> 3% of each run, Pallas kernels for 0% -> 0%
where the time goes in v1:
time: 573 us
  waiting for transfers between devices  511 us (89%)
  matrix products  26.2 us (5%)
  other arithmetic  18.1 us (3%)
  between operations  13.3 us (2%)
    all_gather x1, waiting for transfers between devices, local(): down_full = lax.all_gather(down_weight, 'fs', axis=0, tiled=True)  125 us
    all_gather x1, waiting for transfers between devices, local(): lax.all_gather(up_weight, 'fs', axis=0, tiled=True)  113 us
    all_gather x1, waiting for transfers between devices, local(): lax.all_gather(rounded_partial(conv_out, output_weight).astype(jnp.bfloat...  55.6 us
    all_gather x1, waiting for transfers between devices, local(): lax.all_gather(gate_inner, 'fs', axis=0, tiled=True)  42.3 us
    all_gather x1, waiting for transfers between devices, local(): output_weight = lax.all_gather(mixer_output, 'fs', axis=0, tiled=True)  41 us
    all_gather x1, waiting for transfers between devices, local(): lax.all_gather(gate_outer, 'fs', axis=0, tiled=True)  39.2 us
    all_gather x1, waiting for transfers between devices, local(): lax.all_gather(conv_input, 'fs', axis=0, tiled=True)  38.6 us
    reduce_scatter x1, waiting for transfers between devices, local(): lax.psum_scatter(rounded_partial(hidden, down_full).astype(jnp.bfloat16),...  29.4 us
  transfers between devices with their start and end apart: 9, of which 9 were waited for; matrix products, arithmetic and copies ran while one was open for 3% of the time, Pallas kernels for 0%

profile of v1, /device:TPU:0, one launch (start us, length us, event | category | flops | bytes accessed | tf_op | source)
XLA Modules:
  0.0 572.8 jit_solution(1696427650436035769)
XLA Ops:
  6.5 0.7 all-gather.12.cloned.1.call-update
  7.3 0.7 all-gather.14.cloned.1.call-update
  8.1 0.7 all-gather.10.cloned.1.call-update
  8.8 0.5 all-gather.16.cloned.1.call-update
  9.3 0.0 all-gather.24.cloned.1.call-start
  9.4 0.8 fusion.16
  10.2 42.3 %all-gather.12.cloned.1.call-done = bf16[2048,256]{1,0:T(8,128)(2,1)} async-done(((bf16[256,256]{1,0:T(8,128)(2,1)}), bf16[2048,256]{1,0:T(8,128)(2,1)}) %all-gather.12.cloned.1.call-update) | async-done | bytes 1048592 | tf_op jit(solution)/shard_map/all_gather | solution.py:60
  52.5 2.6 fusion.17
  55.1 38.6 %all-gather.14.cloned.1.call-done = bf16[2048,256]{1,0:T(8,128)(2,1)} async-done(((bf16[256,256]{1,0:T(8,128)(2,1)}), bf16[2048,256]{1,0:T(8,128)(2,1)}) %all-gather.14.cloned.1.call-update) | async-done | bytes 1048592 | tf_op jit(solution)/shard_map/all_gather | solution.py:65
  93.6 1.9 convolution_multiply_fusion
  95.6 39.2 %all-gather.10.cloned.1.call-done = bf16[2048,256]{1,0:T(8,128)(2,1)} async-done(((bf16[256,256]{1,0:T(8,128)(2,1)}), bf16[2048,256]{1,0:T(8,128)(2,1)}) %all-gather.10.cloned.1.call-update) | async-done | bytes 1048592 | tf_op jit(solution)/shard_map/all_gather | solution.py:55
  134.8 41.0 %all-gather.16.cloned.1.call-done = bf16[2048,256]{1,0:T(8,128)(2,1)} async-done(((bf16[256,256]{1,0:T(8,128)(2,1)}), bf16[2048,256]{1,0:T(8,128)(2,1)}) %all-gather.16.cloned.1.call-update) | async-done | bytes 1048592 | tf_op jit(solution)/shard_map/all_gather | solution.py:68
  175.8 5.2 convolution_convert_fusion
  181.0 0.0 all-gather.18.cloned.1.call-start
  181.0 0.5 all-gather.18.cloned.1.call-update
  181.6 0.7 all-gather.20.cloned.1.call-update
  182.3 0.2 reduce-scatter.2.cloned.1.call-start
  182.5 55.6 %all-gather.24.cloned.1.call-done = bf16[2048,2048]{1,0:T(8,128)(2,1)} async-done(((bf16[512,2048]{1,0:T(8,128)(2,1)}), bf16[2048,2048]{1,0:T(8,128)(2,1)}) %all-gather.24.cloned.1.call-update) | async-done | bytes 8388624 | tf_op jit(solution)/shard_map/all_gather | solution.py:71
  238.1 7.2 %reduce_sum.48 = bf16[512,2048]{1,0:T(8,128)(2,1)} reduce(bf16[4,512,2048]{2,1,0:T(8,128)(2,1)} %bitcast.14, bf16[]{:T(256)} %constant.11.clone.1), dimensions={0}, to_apply=%region_0.1 | reduce | flops 3145728 | bytes 10485762 | tf_op jit(solution)/shard_map/reduce_sum | solution.py:70
  245.3 2.5 fusion
  247.8 1.0 multiply_reduce_fusion
  248.9 2.5 add_convert_fusion
  251.4 113.2 %all-gather.18.cloned.1.call-done = bf16[2048,2048]{1,0:T(8,128)(2,1)} async-done(((bf16[256,2048]{1,0:T(8,128)(2,1)}), bf16[2048,2048]{1,0:T(8,128)(2,1)}) %all-gather.18.cloned.1.call-update) | async-done | bytes 8388624 | tf_op jit(solution)/shard_map/all_gather | solution.py:80
  364.6 124.8 %all-gather.20.cloned.1.call-done = bf16[2048,2048]{1,0:T(8,128)(2,1)} async-done(((bf16[256,2048]{1,0:T(8,128)(2,1)}), bf16[2048,2048]{1,0:T(8,128)(2,1)}) %all-gather.20.cloned.1.call-update) | async-done | bytes 8388624 | tf_op jit(solution)/shard_map/all_gather | solution.py:83
  489.4 16.5 %convolution_convert_fusion.1 = bf16[512,2048]{1,0:T(8,128)(2,1)} fusion(bf16[2048,2048]{1,0:T(8,128)(2,1)} %all-gather.20.cloned.1.call-done, bf16[512,2048]{1,0:T(8,128)(2,1)} %add_convert_fusion, bf16[2048,2048]{1,0:T(8,128)(2,1)} %all-gather.18.cloned.1.call-done), kind=kOutput, calls=%fused_computation.6 | convolution fusion | flops 8594128896 | bytes 20971520 | tf_op jit(solution)/shard_map/dot_general | solution.py:18
  506.0 0.0 all-gather.22.cloned.1.call-start
  506.0 29.4 %reduce-scatter.2.cloned.1.call-done = bf16[128,2048]{1,0:T(8,128)(2,1)} async-done(((bf16[512,2048]{1,0:T(8,128)(2,1)}), bf16[128,2048]{1,0:T(8,128)(2,1)}) %reduce-scatter.2.cloned.1.call-update) | async-done | bytes 524304 | tf_op jit(solution)/shard_map/reduce_scatter | solution.py:85
  535.5 1.3 fusion.2
  536.8 1.4 multiply_reduce_fusion.1
  538.2 2.2 add_convert_fusion.1
  540.3 22.7 %all-gather.22.cloned.1.call-done = bf16[512,2048]{1,0:T(8,128)(2,1)} async-done(((bf16[128,2048]{1,0:T(8,128)(2,1)}), bf16[512,2048]{1,0:T(8,128)(2,1)}) %all-gather.22.cloned.1.call-update) | async-done | bytes 2097168 | tf_op jit(solution)/shard_map/all_gather | solution.py:94
  563.1 3.2 copy.14
  (26 shorter events, 0.3 us)
Async XLA Ops:
  6.5 87.1 %copy-start = (bf16[512,2048]{1,0:T(8,128)(2,1)S(1)}, bf16[512,2048]{1,0:T(8,128)(2,1)}, u32[]{:S(2)}) copy-start(bf16[512,2048]{1,0:T(8,128)(2,1)} %param.12) | copy-start | bytes 6291460
  6.5 46.0 %all-gather.12.cloned.1.call-start = ((), (), s32[]{:S(2)}) async-start(), calls=%async_computation.2 | async-start | bytes 1179648 | tf_op jit(solution)/shard_map/all_gather | solution.py:60
  7.3 86.4 %all-gather.14.cloned.1.call-start = ((), (), s32[]{:S(2)}) async-start(), calls=%async_computation.3 | async-start | bytes 1179648 | tf_op jit(solution)/shard_map/all_gather | solution.py:65
  8.0 126.8 %all-gather.10.cloned.1.call-start = ((), (), s32[]{:S(2)}) async-start(), calls=%async_computation.1 | async-start | bytes 1179648 | tf_op jit(solution)/shard_map/all_gather | solution.py:55
  8.7 167.1 %all-gather.16.cloned.1.call-start = ((), (), s32[]{:S(2)}) async-start(), calls=%async_computation.4 | async-start | bytes 1179648 | tf_op jit(solution)/shard_map/all_gather | solution.py:68
  9.3 228.8 %all-gather.24.cloned.1.call-start = ((), (), s32[]{:S(2)}) async-start(), calls=%async_computation.9 | async-start | bytes 10485760 | tf_op jit(solution)/shard_map/all_gather | solution.py:71
  181.0 183.6 %all-gather.18.cloned.1.call-start = ((), (), s32[]{:S(2)}) async-start(), calls=%async_computation.5 | async-start | bytes 9437184 | tf_op jit(solution)/shard_map/all_gather | solution.py:80
  181.6 307.9 %all-gather.20.cloned.1.call-start = ((), (), s32[]{:S(2)}) async-start(), calls=%async_computation.6 | async-start | bytes 9437184 | tf_op jit(solution)/shard_map/all_gather | solution.py:83
  182.3 353.1 %reduce-scatter.2.cloned.1.call-start = ((), (), s32[]{:S(2)}) async-start(), calls=%async_computation.7 | async-start | bytes 2621440 | tf_op jit(solution)/shard_map/reduce_scatter | solution.py:85
  245.3 2.5 copy-start.1
  245.3 3.5 copy-start.3
  245.3 3.6 copy-start.4
  251.4 284.1 %copy-start.2 = (bf16[512,2048]{1,0:T(8,128)(2,1)S(1)}, bf16[512,2048]{1,0:T(8,128)(2,1)}, u32[]{:S(2)}) copy-start(bf16[512,2048]{1,0:T(8,128)(2,1)} %add_convert_fusion) | copy-start | bytes 6291460
  505.9 32.2 %copy-start.5 = (f32[2048]{0:T(1024)S(1)}, f32[2048]{0:T(1024)}, u32[]{:S(2)}) copy-start(f32[2048]{0:T(1024)} %param.23) | copy-start | bytes 24580
  505.9 32.2 %copy-start.6 = (f32[2048]{0:T(1024)S(1)}, f32[2048]{0:T(1024)}, u32[]{:S(2)}) copy-start(f32[2048]{0:T(1024)} %param.22) | copy-start | bytes 24580
  506.0 57.1 %all-gather.22.cloned.1.call-start = ((), (), s32[]{:S(2)}) async-start(), calls=%async_computation.8 | async-start | bytes 2621440 | tf_op jit(solution)/shard_map/all_gather | solution.py:94
Sparse Core Ops, SparseCore 0:
  9.5 42.9 all-gather.11
  54.6 38.9 all-gather.13
  95.8 38.9 all-gather.9
  136.8 38.9 all-gather.15
  181.1 56.9 all-gather.23
  240.1 124.4 all-gather.17
  366.7 122.6 all-gather.19
  506.1 29.3 reduce-scatter.1
  540.5 22.5 all-gather.21
